TPU v7x, 512 devices: a whole 4x4x16 slice. The times are simulated.
512 devices in a mesh: sp: 16 (over z), dp: 32 (over y, x, core).
Axes of the slice: x: 4, y: 4, z: 16, core: 2. Of those that a mesh axis runs over, the one named last changes fastest.
Arguments:
- inputs: bfloat16 [32, 2176, 2048], P('dp', 'sp'), may hold values from -6 to 6
- query_vectors: bfloat16 [32, 2176, 1024], P('dp', 'sp'), may hold values from -6 to 6
- key_vectors: bfloat16 [32, 2176, 1024], P('dp', 'sp'), may hold values from -6 to 6
- value_vectors: bfloat16 [32, 2176, 1024], P('dp', 'sp'), may hold values from -6 to 6
- cotangent: bfloat16 [32, 2176, 1024], P('dp', 'sp'), may hold values from -6 to 6
- gate_prefix: float32 [32, 16, 2176], P('dp', 'sp'), may hold values from -2176 to 0, as said below
- value_weight: bfloat16 [2048, 1024], P('sp', 'dp'), may hold values from -0.125 to 0.125
Outputs:
- query_grad: bfloat16 [32, 2176, 1024], P('dp', 'sp')
- key_grad: bfloat16 [32, 2176, 1024], P('dp', 'sp')
- input_grad: bfloat16 [32, 2176, 2048], P('dp', 'sp')
- weight_grad: float32 [2048, 1024], P('sp', 'dp')
Inputs may be any that keep to these rules, and one draw needn't show every extreme that they name: `gate_prefix`: non-increasing along the positions of each sequence and head.
All inputs are finite; a program needn't handle non-finite values.
Results may differ from a plain program's by a relative error of at most 0.015.
Values may be sent and summed in bfloat16 or wider, within the bound.
No kernel may reach another device: no remote copies, remote signals or barrier semaphores. Data moves between devices by JAX's collectives and lax.ppermute only.
A program may use at most 128 MiB of HBM per device.

v0:
```python
import jax
import jax.numpy as jnp
from jax import lax
from jax.sharding import PartitionSpec as P

HEAD_DIM = 64


def in_order(blocks, dim):
    lengths = list(blocks.shape[1:])
    lengths[dim] *= blocks.shape[0]
    return jnp.moveaxis(blocks, 0, dim).reshape(lengths)


def sent_to_all(shard, axis):
    copies = jnp.broadcast_to(shard, (lax.axis_size(axis), *shard.shape))
    return lax.all_to_all(copies, axis, split_axis=0, concat_axis=0, tiled=True)


def gather_directly(shard, axis, dim):
    return in_order(sent_to_all(shard, axis), dim)


def cut_along(shard, dim, peers):
    lengths = shard.shape
    blocks = shard.reshape(*lengths[:dim], peers, lengths[dim] // peers, *lengths[dim + 1 :])
    return jnp.moveaxis(blocks, dim, 0)


def summed_on_arrival(shard, axis, dim):
    blocks = cut_along(shard, dim, lax.axis_size(axis))
    arrived = lax.all_to_all(blocks, axis, split_axis=0, concat_axis=0, tiled=True)
    return arrived.astype(jnp.float32).sum(axis=0)


def attention_backward(query_heads, key_heads, value_heads, grad_heads, prefix):
    length = query_heads.shape[0]
    score_scale = HEAD_DIM ** (-0.5)
    block_count = max(1, length // 512)
    block_rows = length // block_count
    key_accum = jnp.zeros(key_heads.shape, jnp.float32)
    value_accum = jnp.zeros(key_heads.shape, jnp.float32)
    query_parts = []
    for block_index in range(block_count):
        first_row = block_index * block_rows
        last_row = first_row + block_rows
        query_rows = query_heads[first_row:last_row]
        key_rows = key_heads[:last_row]
        grad_rows = grad_heads[first_row:last_row]
        scores = (
            jnp.einsum("qhd,khd->hqk", query_rows, key_rows, preferred_element_type=jnp.float32)
            * score_scale
        )
        scores = scores + prefix[:, first_row:last_row, None] - prefix[:, None, :last_row]
        causal = jnp.arange(last_row)[None, :] <= (first_row + jnp.arange(block_rows))[:, None]
        scores = jnp.where(causal[None], scores, -jnp.inf)
        row_peak = jnp.max(scores, axis=-1, keepdims=True)
        raised_scores = jnp.exp(scores - row_peak)
        softmax_rows = raised_scores / jnp.sum(raised_scores, axis=-1, keepdims=True)
        softmax_low = softmax_rows.astype(jnp.bfloat16)
        value_accum = value_accum.at[:last_row].add(
            jnp.einsum("hqk,qhd->khd", softmax_low, grad_rows, preferred_element_type=jnp.float32)
        )
        softmax_grad = jnp.einsum(
            "qhd,khd->hqk", grad_rows, value_heads[:last_row], preferred_element_type=jnp.float32
        )
        row_term = jnp.sum(softmax_rows * softmax_grad, axis=-1, keepdims=True)
        score_low = (softmax_rows * (softmax_grad - row_term)).astype(jnp.bfloat16)
        query_parts.append(
            (
                jnp.einsum("hqk,khd->qhd", score_low, key_rows, preferred_element_type=jnp.float32)
                * score_scale
            ).astype(jnp.bfloat16)
        )
        key_accum = key_accum.at[:last_row].add(
            jnp.einsum("hqk,qhd->khd", score_low, query_rows, preferred_element_type=jnp.float32)
        )
    query_grad = jnp.concatenate(query_parts, axis=0)
    key_grad = (key_accum * score_scale).astype(jnp.bfloat16)
    return (query_grad, key_grad, value_accum.astype(jnp.bfloat16))


def shards(inputs, query_vectors, key_vectors, value_vectors, cotangent, gate_prefix, value_weight):
    query_seq, key_seq, value_seq, grad_seq, input_cols = (
        lax.all_to_all(query_vectors[0], "sp", split_axis=1, concat_axis=0, tiled=True),
        lax.all_to_all(key_vectors[0], "sp", split_axis=1, concat_axis=0, tiled=True),
        lax.all_to_all(value_vectors[0], "sp", split_axis=1, concat_axis=0, tiled=True),
        lax.all_to_all(cotangent[0], "sp", split_axis=1, concat_axis=0, tiled=True),
        lax.all_to_all(inputs[0], "sp", split_axis=1, concat_axis=0, tiled=True),
    )
    length = query_seq.shape[0]
    local_width = query_seq.shape[1]
    head_shape = (length, local_width // HEAD_DIM, HEAD_DIM)
    query_heads, key_heads, value_heads = attention_backward(
        query_seq.reshape(head_shape),
        key_seq.reshape(head_shape),
        value_seq.reshape(head_shape),
        grad_seq.reshape(head_shape),
        gate_prefix[0],
    )
    query_flat = query_heads.reshape(length, local_width)
    key_flat = key_heads.reshape(length, local_width)
    value_flat = value_heads.reshape(length, local_width)
    value_all = lax.all_gather(value_flat, "sp", axis=1, tiled=True)
    weight_block = gather_directly(value_weight, "dp", 1)
    weight_rows = summed_on_arrival(
        lax.dot_general(
            value_all, input_cols, (((0,), (0,)), ((), ())), preferred_element_type=jnp.float32
        ).astype(jnp.bfloat16),
        "dp",
        0,
    )
    weight_grad = weight_rows.T
    query_back, key_back = (
        lax.all_to_all(query_flat, "sp", split_axis=0, concat_axis=1, tiled=True),
        lax.all_to_all(key_flat, "sp", split_axis=0, concat_axis=1, tiled=True),
    )
    column_grad = lax.dot_general(
        value_all, weight_block, (((1,), (1,)), ((), ())), preferred_element_type=jnp.float32
    ).astype(jnp.bfloat16)
    input_grad = lax.all_to_all(column_grad, "sp", split_axis=0, concat_axis=1, tiled=True)
    return (query_back[None], key_back[None], input_grad[None], weight_grad)


def solution(mesh):
    in_specs = (
        P("dp", "sp", None),
        P("dp", "sp", None),
        P("dp", "sp", None),
        P("dp", "sp", None),
        P("dp", "sp", None),
        P("dp", "sp", None),
        P("sp", "dp"),
    )
    out_specs = (P("dp", "sp", None), P("dp", "sp", None), P("dp", "sp", None), P("sp", "dp"))
    return jax.shard_map(shards, mesh=mesh, in_specs=in_specs, out_specs=out_specs, check_vma=False)
```

profile of v0, /device:TPU:32, one launch (start us, length us, event | category | flops | bytes accessed | tf_op | source)
XLA Modules:
  0.0 370.8 jit_solution(8729576599955904067)
XLA Ops:
  9.2 15.3 %all-to-all-start = ((bf16[136,16,64]{0,2,1:T(8,128)(2,1)}), bf16[136,16,64]{0,2,1:T(8,128)(2,1)S(1)}, u32[]{:S(2)}, u32[]{:S(2)}) async-start(bf16[136,16,64]{0,2,1:T(8,128)(2,1)} %bitcast), calls=%async_computation | async-start | bytes 1048576 | tf_op jit(solution)/shard_map/all_to_all | solution.py:85
  26.5 26.5 %all-to-all-done = bf16[136,16,64]{0,2,1:T(8,128)(2,1)S(1)} async-done(((bf16[136,16,64]{0,2,1:T(8,128)(2,1)}), bf16[136,16,64]{0,2,1:T(8,128)(2,1)S(1)}, u32[]{:S(2)}, u32[]{:S(2)}) %all-to-all-start) | async-done | bytes 278560 | tf_op jit(solution)/shard_map/all_to_all | solution.py:85
  53.0 6.9 %all-to-all-start.1 = ((bf16[136,16,64]{0,2,1:T(8,128)(2,1)}), bf16[136,16,64]{0,2,1:T(8,128)(2,1)S(1)}, u32[]{:S(2)}, u32[]{:S(2)}) async-start(bf16[136,16,64]{0,2,1:T(8,128)(2,1)} %bitcast.2), calls=%async_computation.1 | async-start | bytes 1048576 | tf_op jit(solution)/shard_map/all_to_all | solution.py:86
  60.9 27.5 %all-to-all-done.1 = bf16[136,16,64]{0,2,1:T(8,128)(2,1)S(1)} async-done(((bf16[136,16,64]{0,2,1:T(8,128)(2,1)}), bf16[136,16,64]{0,2,1:T(8,128)(2,1)S(1)}, u32[]{:S(2)}, u32[]{:S(2)}) %all-to-all-start.1) | async-done | bytes 278560 | tf_op jit(solution)/shard_map/all_to_all | solution.py:86
  88.4 6.9 %all-to-all-start.2 = ((bf16[136,16,64]{0,2,1:T(8,128)(2,1)}), bf16[136,16,64]{0,2,1:T(8,128)(2,1)S(1)}, u32[]{:S(2)}, u32[]{:S(2)}) async-start(bf16[136,16,64]{0,2,1:T(8,128)(2,1)} %bitcast.5), calls=%async_computation.2 | async-start | bytes 1048576 | tf_op jit(solution)/shard_map/all_to_all | solution.py:88
  104.4 19.5 %all-to-all-done.2 = bf16[136,16,64]{0,2,1:T(8,128)(2,1)S(1)} async-done(((bf16[136,16,64]{0,2,1:T(8,128)(2,1)}), bf16[136,16,64]{0,2,1:T(8,128)(2,1)S(1)}, u32[]{:S(2)}, u32[]{:S(2)}) %all-to-all-start.2) | async-done | bytes 278560 | tf_op jit(solution)/shard_map/all_to_all | solution.py:88
  123.9 6.9 %all-to-all-start.3 = ((bf16[136,16,64]{0,2,1:T(8,128)(2,1)}), bf16[136,16,64]{0,2,1:T(8,128)(2,1)S(1)}, u32[]{:S(2)}, u32[]{:S(2)}) async-start(bf16[136,16,64]{0,2,1:T(8,128)(2,1)} %bitcast.7), calls=%async_computation.3 | async-start | bytes 1048576 | tf_op jit(solution)/shard_map/all_to_all | solution.py:87
  144.8 3.7 fusion.26
  148.5 3.3 scatter-add.29
  160.7 7.7 %all-to-all-start.6 = ((bf16[32,128,32]{1,2,0:T(8,128)(2,1)}), bf16[32,128,32]{1,2,0:T(8,128)(2,1)}, u32[]{:S(2)}, u32[]{:S(2)}) async-start(bf16[32,128,32]{1,2,0:T(8,128)(2,1)} %broadcast_in_dim.29), calls=%async_computation.6 | async-start | bytes 524288 | tf_op jit(solution)/shard_map/all_to_all | solution.py:17
  184.4 12.1 %all-to-all-start.8 = ((bf16[136,16,128]{2,0,1:T(8,128)(2,1)}), bf16[136,16,128]{2,0,1:T(8,128)(2,1)}, u32[]{:S(2)}, u32[]{:S(2)}) async-start(bf16[136,16,128]{2,0,1:T(8,128)(2,1)} %copy.79), calls=%async_computation.8 | async-start | bytes 1114112 | tf_op jit(solution)/shard_map/all_to_all | solution.py:89
  196.5 3.8 %multiply_reduce_fusion = (f32[544]{0:T(1024)S(1)}, f32[544,2176]{1,0:T(8,128)S(1)}) fusion(f32[544]{0:T(1024)S(1)} %copy-done.40, f32[544,2176]{1,0:T(8,128)} %copy-done, f32[544]{0:T(1024)S(1)} %copy-done.38, bf16[544,64]{0,1:T(8,128)(2,1)S(1)} %copy-done.30, bf16[2176,64]{0,1:T(8,128)(2,1)S(1)} %reshape.635), kind=kOutput, calls=%fused_computation.5 | convolution fusion | flops 156253664 | bytes 9824640 | tf_op jit(solution)/shard_map/qhd,khd->hqk/dot_general | solution.py:64
  210.5 22.6 %all-to-all-done.8 = bf16[136,16,128]{2,0,1:T(8,128)(2,1)} async-done(((bf16[136,16,128]{2,0,1:T(8,128)(2,1)}), bf16[136,16,128]{2,0,1:T(8,128)(2,1)}, u32[]{:S(2)}, u32[]{:S(2)}) %all-to-all-start.8) | async-done | bytes 557088 | tf_op jit(solution)/shard_map/all_to_all | solution.py:89
  233.1 6.8 %all-to-all-start.4 = ((bf16[16,136,64]{1,2,0:T(8,128)(2,1)}), bf16[16,136,64]{1,2,0:T(8,128)(2,1)}, u32[]{:S(2)}, u32[]{:S(2)}) async-start(bf16[16,136,64]{1,2,0:T(8,128)(2,1)} %copy.74), calls=%async_computation.4 | async-start | bytes 1048576 | tf_op jit(solution)/shard_map/all_to_all | solution.py:115
  245.3 3.2 scatter-add.24
  251.4 23.1 %all-to-all-done.4 = bf16[16,136,64]{1,2,0:T(8,128)(2,1)} async-done(((bf16[16,136,64]{1,2,0:T(8,128)(2,1)}), bf16[16,136,64]{1,2,0:T(8,128)(2,1)}, u32[]{:S(2)}, u32[]{:S(2)}) %all-to-all-start.4) | async-done | bytes 278560 | tf_op jit(solution)/shard_map/all_to_all | solution.py:115
  274.4 6.7 %all-to-all-start.5 = ((bf16[16,136,64]{1,2,0:T(8,128)(2,1)}), bf16[16,136,64]{1,2,0:T(8,128)(2,1)S(1)}, u32[]{:S(2)}, u32[]{:S(2)}) async-start(bf16[16,136,64]{1,2,0:T(8,128)(2,1)} %copy.76), calls=%async_computation.5 | async-start | bytes 1048576 | tf_op jit(solution)/shard_map/all_to_all | solution.py:116
  281.2 4.4 %fusion.36 = bf16[1024,128]{1,0:T(8,128)(2,1)} fusion(bf16[2176,128]{1,0:T(8,128)(2,1)} %bitcast.55, bf16[2176,1,1024]{0,2,1:T(8,128)(2,1)} %all-gather.3.cloned.1.call-done), kind=kOutput, calls=%fused_computation.60 | convolution fusion | flops 570556416 | bytes 5275648 | tf_op jit(solution)/shard_map/dot_general | solution.py:107
  285.6 23.5 %all-to-all-done.5 = bf16[16,136,64]{1,2,0:T(8,128)(2,1)S(1)} async-done(((bf16[16,136,64]{1,2,0:T(8,128)(2,1)}), bf16[16,136,64]{1,2,0:T(8,128)(2,1)S(1)}, u32[]{:S(2)}, u32[]{:S(2)}) %all-to-all-start.5) | async-done | bytes 278560 | tf_op jit(solution)/shard_map/all_to_all | solution.py:116
  309.1 6.9 %all-to-all-start.9 = ((bf16[32,32,128]{2,1,0:T(8,128)(2,1)}), bf16[32,32,128]{2,1,0:T(8,128)(2,1)S(1)}, u32[]{:S(2)}, u32[]{:S(2)}) async-start(bf16[32,32,128]{2,1,0:T(8,128)(2,1)} %bitcast.56), calls=%async_computation.9 | async-start | bytes 524288 | tf_op jit(solution)/shard_map/all_to_all | solution.py:32
  316.0 4.5 %fusion.9 = bf16[2176,128]{1,0:T(8,128)(2,1)} fusion(bf16[128,1024]{0,1:T(8,128)(2,1)} %bitcast.51, bf16[2176,1,1024]{0,2,1:T(8,128)(2,1)} %all-gather.3.cloned.1.call-done), kind=kOutput, calls=%fused_computation.19 | convolution fusion | flops 570703872 | bytes 5275648 | tf_op jit(solution)/shard_map/dot_general | solution.py:118
  320.5 4.3 %all-to-all-done.9 = bf16[32,32,128]{2,1,0:T(8,128)(2,1)S(1)} async-done(((bf16[32,32,128]{2,1,0:T(8,128)(2,1)}), bf16[32,32,128]{2,1,0:T(8,128)(2,1)S(1)}, u32[]{:S(2)}, u32[]{:S(2)}) %all-to-all-start.9) | async-done | bytes 262176 | tf_op jit(solution)/shard_map/all_to_all | solution.py:32
  324.8 7.1 %all-to-all-start.7 = ((bf16[16,136,128]{2,1,0:T(8,128)(2,1)}), bf16[16,136,128]{2,1,0:T(8,128)(2,1)S(1)}, u32[]{:S(2)}, u32[]{:S(2)}) async-start(bf16[16,136,128]{2,1,0:T(8,128)(2,1)} %bitcast.52), calls=%async_computation.7 | async-start | bytes 1114112 | tf_op jit(solution)/shard_map/all_to_all | solution.py:121
  335.3 27.5 %all-to-all-done.7 = bf16[16,136,128]{2,1,0:T(8,128)(2,1)S(1)} async-done(((bf16[16,136,128]{2,1,0:T(8,128)(2,1)}), bf16[16,136,128]{2,1,0:T(8,128)(2,1)S(1)}, u32[]{:S(2)}, u32[]{:S(2)}) %all-to-all-start.7) | async-done | bytes 557088 | tf_op jit(solution)/shard_map/all_to_all | solution.py:121
  (219 shorter events, 75.3 us)
Async XLA Ops:
  7.2 52.8 %copy-start.25 = (bf16[1,136,1024]{2,1,0:T(8,128)(2,1)S(1)}, bf16[1,136,1024]{2,1,0:T(8,128)(2,1)}, u32[]{:S(2)}) copy-start(bf16[1,136,1024]{2,1,0:T(8,128)(2,1)} %param.31) | copy-start | bytes 835588
  9.2 86.2 %copy-start.26 = (bf16[1,136,1024]{2,1,0:T(8,128)(2,1)S(1)}, bf16[1,136,1024]{2,1,0:T(8,128)(2,1)}, u32[]{:S(2)}) copy-start(bf16[1,136,1024]{2,1,0:T(8,128)(2,1)} %param.30) | copy-start | bytes 835588
  9.2 43.8 %all-to-all-start = ((bf16[136,16,64]{0,2,1:T(8,128)(2,1)}), bf16[136,16,64]{0,2,1:T(8,128)(2,1)S(1)}, u32[]{:S(2)}, u32[]{:S(2)}) async-start(bf16[136,16,64]{0,2,1:T(8,128)(2,1)} %bitcast), calls=%async_computation | async-start | bytes 1048576 | tf_op jit(solution)/shard_map/all_to_all | solution.py:85
  24.5 71.8 %copy-start.28 = (f32[1,1,2176]{2,1,0:T(1,128)S(1)}, f32[1,1,2176]{2,1,0:T(1,128)}, u32[]{:S(2)}) copy-start(f32[1,1,2176]{2,1,0:T(1,128)} %param.32) | copy-start | bytes 26116
  53.0 35.4 %all-to-all-start.1 = ((bf16[136,16,64]{0,2,1:T(8,128)(2,1)}), bf16[136,16,64]{0,2,1:T(8,128)(2,1)S(1)}, u32[]{:S(2)}, u32[]{:S(2)}) async-start(bf16[136,16,64]{0,2,1:T(8,128)(2,1)} %bitcast.2), calls=%async_computation.1 | async-start | bytes 1048576 | tf_op jit(solution)/shard_map/all_to_all | solution.py:86
  88.4 35.5 %all-to-all-start.2 = ((bf16[136,16,64]{0,2,1:T(8,128)(2,1)}), bf16[136,16,64]{0,2,1:T(8,128)(2,1)S(1)}, u32[]{:S(2)}, u32[]{:S(2)}) async-start(bf16[136,16,64]{0,2,1:T(8,128)(2,1)} %bitcast.5), calls=%async_computation.2 | async-start | bytes 1048576 | tf_op jit(solution)/shard_map/all_to_all | solution.py:88
  101.6 32.3 %copy-start.22 = (bf16[544,64]{0,1:T(8,128)(2,1)}, bf16[544,64]{0,1:T(8,128)(2,1)S(1)}, u32[]{:S(2)}) copy-start(bf16[544,64]{0,1:T(8,128)(2,1)S(1)} %reshape.620) | copy-start | bytes 208900
  101.9 32.1 %copy-start.23 = (bf16[544,64]{0,1:T(8,128)(2,1)}, bf16[544,64]{0,1:T(8,128)(2,1)S(1)}, u32[]{:S(2)}) copy-start(bf16[544,64]{0,1:T(8,128)(2,1)S(1)} %reshape.621) | copy-start | bytes 208900
  103.6 48.2 %copy-start.9 = (bf16[2176,64]{0,1:T(8,128)(2,1)}, bf16[2176,64]{0,1:T(8,128)(2,1)S(1)}, u32[]{:S(2)}) copy-start(bf16[2176,64]{0,1:T(8,128)(2,1)S(1)} %reshape.633) | copy-start | bytes 835588
  103.9 30.1 %copy-start.59 = (f32[544]{0:T(1024)S(1)}, f32[544]{0:T(1024)}, u32[]{:S(2)}) copy-start(f32[544]{0:T(1024)} %get-tuple-element.119) | copy-start | bytes 6532
  104.4 34.7 %copy-start.11 = (bf16[1632,64]{0,1:T(8,128)(2,1)}, bf16[1632,64]{0,1:T(8,128)(2,1)S(1)}, u32[]{:S(2)}) copy-start(bf16[1632,64]{0,1:T(8,128)(2,1)S(1)} %reshape.629) | copy-start | bytes 626692
  123.9 36.0 %all-to-all-start.3 = ((bf16[136,16,64]{0,2,1:T(8,128)(2,1)}), bf16[136,16,64]{0,2,1:T(8,128)(2,1)S(1)}, u32[]{:S(2)}, u32[]{:S(2)}) async-start(bf16[136,16,64]{0,2,1:T(8,128)(2,1)} %bitcast.7), calls=%async_computation.3 | async-start | bytes 1048576 | tf_op jit(solution)/shard_map/all_to_all | solution.py:87
  130.8 150.4 %all-gather.3.cloned.1.call-start = ((), (), s32[]{:S(2)}) async-start(), calls=%async_computation.10 | async-start | bytes 4734976 | tf_op jit(solution)/shard_map/all_gather | solution.py:104
  160.7 23.7 %all-to-all-start.6 = ((bf16[32,128,32]{1,2,0:T(8,128)(2,1)}), bf16[32,128,32]{1,2,0:T(8,128)(2,1)}, u32[]{:S(2)}, u32[]{:S(2)}) async-start(bf16[32,128,32]{1,2,0:T(8,128)(2,1)} %broadcast_in_dim.29), calls=%async_computation.6 | async-start | bytes 524288 | tf_op jit(solution)/shard_map/all_to_all | solution.py:17
  182.1 14.4 %copy-start.38 = (f32[544]{0:T(1024)S(1)}, f32[544]{0:T(1024)}, u32[]{:S(2)}) copy-start(f32[544]{0:T(1024)} %copy-done.37) | copy-start | bytes 6532
  182.1 14.4 %copy-start.40 = (f32[544]{0:T(1024)S(1)}, f32[544]{0:T(1024)}, u32[]{:S(2)}) copy-start(f32[544]{0:T(1024)} %copy-done.39) | copy-start | bytes 6532
  184.4 48.7 %all-to-all-start.8 = ((bf16[136,16,128]{2,0,1:T(8,128)(2,1)}), bf16[136,16,128]{2,0,1:T(8,128)(2,1)}, u32[]{:S(2)}, u32[]{:S(2)}) async-start(bf16[136,16,128]{2,0,1:T(8,128)(2,1)} %copy.79), calls=%async_computation.8 | async-start | bytes 1114112 | tf_op jit(solution)/shard_map/all_to_all | solution.py:89
  205.0 34.9 %copy-start.6 = (bf16[544,544]{0,1:T(8,128)(2,1)S(1)}, bf16[544,544]{0,1:T(8,128)(2,1)}, u32[]{:S(2)}) copy-start(bf16[544,544]{0,1:T(8,128)(2,1)} %copy-done.5) | copy-start | bytes 1775620
  205.0 36.2 %copy-start.17 = (bf16[544,64]{0,1:T(8,128)(2,1)S(1)}, bf16[544,64]{0,1:T(8,128)(2,1)}, u32[]{:S(2)}) copy-start(bf16[544,64]{0,1:T(8,128)(2,1)} %reshape.624) | copy-start | bytes 208900
  210.5 32.8 %copy-start.21 = (bf16[544,64]{0,1:T(8,128)(2,1)S(1)}, bf16[544,64]{0,1:T(8,128)(2,1)}, u32[]{:S(2)}) copy-start(bf16[544,64]{0,1:T(8,128)(2,1)} %reshape.628) | copy-start | bytes 208900
  233.1 41.4 %all-to-all-start.4 = ((bf16[16,136,64]{1,2,0:T(8,128)(2,1)}), bf16[16,136,64]{1,2,0:T(8,128)(2,1)}, u32[]{:S(2)}, u32[]{:S(2)}) async-start(bf16[16,136,64]{1,2,0:T(8,128)(2,1)} %copy.74), calls=%async_computation.4 | async-start | bytes 1048576 | tf_op jit(solution)/shard_map/all_to_all | solution.py:115
  274.4 34.7 %all-to-all-start.5 = ((bf16[16,136,64]{1,2,0:T(8,128)(2,1)}), bf16[16,136,64]{1,2,0:T(8,128)(2,1)S(1)}, u32[]{:S(2)}, u32[]{:S(2)}) async-start(bf16[16,136,64]{1,2,0:T(8,128)(2,1)} %copy.76), calls=%async_computation.5 | async-start | bytes 1048576 | tf_op jit(solution)/shard_map/all_to_all | solution.py:116
  309.1 15.7 %all-to-all-start.9 = ((bf16[32,32,128]{2,1,0:T(8,128)(2,1)}), bf16[32,32,128]{2,1,0:T(8,128)(2,1)S(1)}, u32[]{:S(2)}, u32[]{:S(2)}) async-start(bf16[32,32,128]{2,1,0:T(8,128)(2,1)} %bitcast.56), calls=%async_computation.9 | async-start | bytes 524288 | tf_op jit(solution)/shard_map/all_to_all | solution.py:32
  324.8 38.1 %all-to-all-start.7 = ((bf16[16,136,128]{2,1,0:T(8,128)(2,1)}), bf16[16,136,128]{2,1,0:T(8,128)(2,1)S(1)}, u32[]{:S(2)}, u32[]{:S(2)}) async-start(bf16[16,136,128]{2,1,0:T(8,128)(2,1)} %bitcast.52), calls=%async_computation.7 | async-start | bytes 1114112 | tf_op jit(solution)/shard_map/all_to_all | solution.py:121
  (47 other events, 124.3 us)
Sparse Core Ops, SparseCore 0:
  157.9 122.4 all-gather.2
where the time goes:
time: 372 us; the launch traced here: 371 us
  waiting for transfers between devices  175 us (47%)
  starting transfers between devices  83.4 us (22%)
  local copies, waits for them, and re-layouts  52 us (14%)
  matrix products  36.8 us (10%)
  between operations  14.9 us (4%)
  other arithmetic  9.09 us (2%)
    all_to_all x1, waiting for transfers between devices, shards(): lax.all_to_all(column_grad, 'sp', split_axis=0, concat_axis=1, tiled=True)  27.5 us
    all_to_all x1, waiting for transfers between devices, shards(): lax.all_to_all(key_vectors[0], 'sp', split_axis=1, concat_axis=0, tiled=T...  27.5 us
    all_to_all x1, waiting for transfers between devices, shards(): lax.all_to_all(query_vectors[0], 'sp', split_axis=1, concat_axis=0, tiled...  26.5 us
    all_to_all x1, waiting for transfers between devices, shards(): lax.all_to_all(key_flat, 'sp', split_axis=0, concat_axis=1, tiled=True)  23.5 us
    all_to_all x1, waiting for transfers between devices, shards(): lax.all_to_all(query_flat, 'sp', split_axis=0, concat_axis=1, tiled=True)  23.1 us
    all_to_all x1, waiting for transfers between devices, shards(): lax.all_to_all(inputs[0], 'sp', split_axis=1, concat_axis=0, tiled=True)  22.6 us
    all_to_all x1, waiting for transfers between devices, shards(): lax.all_to_all(cotangent[0], 'sp', split_axis=1, concat_axis=0, tiled=True)  19.5 us
    all_to_all x1, starting transfers between devices, shards(): lax.all_to_all(query_vectors[0], 'sp', split_axis=1, concat_axis=0, tiled...  15.3 us
  transfers between devices with their start and end apart: 11, of which 8 were waited for; matrix products, arithmetic and copies ran while one was open for 23% of the time, Pallas kernels for 0%

commit v1 on v0

v1 whole, which is shorter than its diff:
```python
import jax
import jax.numpy as jnp
from jax import lax
from jax.experimental import pallas as pl
from jax.experimental.pallas import tpu as pltpu
from jax.sharding import Mesh, PartitionSpec as P

HEAD_DIM = 64
LANES = 128
TILE = 256
FLOOR = -1e30


def rolled(x):
    return pltpu.roll(x, HEAD_DIM, 1)


def low_lanes(shape):
    return lax.broadcasted_iota(jnp.int32, shape, 1) < HEAD_DIM


def pack_kernel(q_ref, k_ref, v_ref, g_ref, w_ref, out_ref):
    heads, rows, _ = out_ref.shape
    tokens = q_ref.shape[0]
    low = low_lanes((tokens, LANES))
    half = w_ref.shape[0] // 2
    for pair in range(heads // 2):
        cols = slice(pair * LANES, (pair + 1) * LANES)
        for first_ref, second_ref, lane in ((q_ref, k_ref, 0), (v_ref, g_ref, LANES)):
            first = first_ref[:, cols].astype(jnp.float32)
            second = second_ref[:, cols].astype(jnp.float32)
            out_ref[2 * pair, :tokens, lane : lane + LANES] = jnp.where(
                low, first, rolled(second)
            ).astype(jnp.bfloat16)
            out_ref[2 * pair + 1, :tokens, lane : lane + LANES] = jnp.where(
                low, rolled(first), second
            ).astype(jnp.bfloat16)
    for head in range(heads):
        out_ref[head, tokens:rows, :LANES] = w_ref[:half]
        out_ref[head, tokens:rows, LANES:] = w_ref[half:]


def unpack_weight_kernel(x_ref, out_ref):
    planes, half, _ = x_ref.shape
    for plane in range(planes):
        cols = slice(plane * LANES, (plane + 1) * LANES)
        out_ref[:half, cols] = x_ref[plane, :, :LANES]
        out_ref[half:, cols] = x_ref[plane, :, LANES:]


def dot_nt(a, b):
    return lax.dot_general(a, b, (((1,), (1,)), ((), ())), preferred_element_type=jnp.float32)


def dot_nn(a, b):
    return lax.dot_general(a, b, (((1,), (0,)), ((), ())), preferred_element_type=jnp.float32)


def folded(x, op):
    return op(x.reshape(x.shape[0] // 8, 8, x.shape[1]), axis=0)


def attention_kernel(
    x_ref, p_ref, qk_ref, v_out_ref, kq_ref, kt_ref, pc_ref, acc_ref, dq_ref, s_ref, d_ref
):
    length = x_ref.shape[0]
    scale = HEAD_DIM**-0.5
    blocks = [(b, min(TILE, length - b)) for b in range(0, length, TILE)]
    for base, rows in blocks:
        here = slice(base, base + rows)
        wide = x_ref[here, :LANES].astype(jnp.float32)
        swapped = rolled(wide)
        kq_ref[here] = swapped.astype(jnp.bfloat16)
        kt_ref[:, here] = swapped.T[:HEAD_DIM].astype(jnp.bfloat16)
        pc_ref[here] = jnp.broadcast_to(p_ref[:, here], (LANES, rows)).T
        acc_ref[here] = jnp.zeros((rows, LANES), jnp.float32)
    for index, (q_base, q_rows) in enumerate(blocks):
        q_here = slice(q_base, q_base + q_rows)
        low = low_lanes((q_rows, LANES))
        query_wide = x_ref[q_here, :LANES].astype(jnp.float32)
        grad_wide = rolled(x_ref[q_here, LANES:].astype(jnp.float32))
        query_low = jnp.where(low, query_wide * scale, 0.0).astype(jnp.bfloat16)
        query_high = jnp.where(low, 0.0, rolled(query_wide)).astype(jnp.bfloat16)
        grad_low = jnp.where(low, grad_wide, 0.0).astype(jnp.bfloat16)
        pivot = pc_ref[q_base : q_base + 1, :]
        peak = jnp.full((8, q_rows), FLOOR, jnp.float32)
        for u_base, u_rows in blocks[: index + 1]:
            u_here = slice(u_base, u_base + u_rows)
            shift = pivot - pc_ref[u_here]
            shift = jnp.concatenate([shift] * (q_rows // LANES), axis=1)
            scores = dot_nt(kq_ref[u_here], query_low) + shift
            if u_base == q_base:
                seen = lax.broadcasted_iota(jnp.int32, scores.shape, 0) <= lax.broadcasted_iota(
                    jnp.int32, scores.shape, 1
                )
                scores = jnp.where(seen, scores, FLOOR)
            s_ref[u_here, :q_rows] = scores
            peak = jnp.maximum(peak, folded(scores, jnp.max))
        peak = jnp.max(peak, axis=0, keepdims=True)
        total = jnp.zeros((8, q_rows), jnp.float32)
        for u_base, u_rows in blocks[: index + 1]:
            u_here = slice(u_base, u_base + u_rows)
            raised = jnp.exp(s_ref[u_here, :q_rows] - peak)
            s_ref[u_here, :q_rows] = raised
            total = total + folded(raised, jnp.sum)
        share = 1.0 / jnp.sum(total, axis=0, keepdims=True)
        term = jnp.zeros((8, q_rows), jnp.float32)
        for u_base, u_rows in blocks[: index + 1]:
            u_here = slice(u_base, u_base + u_rows)
            soft = s_ref[u_here, :q_rows] * share
            s_ref[u_here, :q_rows] = soft
            acc_ref[u_here] += dot_nn(soft.astype(jnp.bfloat16), grad_low)
            soft_grad = dot_nt(x_ref[u_here, LANES:], grad_low)
            d_ref[u_here, :q_rows] = soft_grad
            term = term + folded(soft * soft_grad, jnp.sum)
        term = jnp.sum(term, axis=0, keepdims=True)
        query_grad = jnp.zeros((HEAD_DIM, q_rows), jnp.float32)
        for u_base, u_rows in blocks[: index + 1]:
            u_here = slice(u_base, u_base + u_rows)
            score_low = (s_ref[u_here, :q_rows] * (d_ref[u_here, :q_rows] - term)).astype(
                jnp.bfloat16
            )
            acc_ref[u_here] += dot_nn(score_low, query_high)
            query_grad = query_grad + dot_nn(kt_ref[:, u_here], score_low)
        query_grad = jnp.concatenate([query_grad, jnp.zeros_like(query_grad)], axis=0)
        dq_ref[q_here] = query_grad.T
    for base, rows in blocks:
        here = slice(base, base + rows)
        qk_ref[here] = (
            jnp.where(low_lanes((rows, LANES)), dq_ref[here], acc_ref[here]) * scale
        ).astype(jnp.bfloat16)
    planes, kept, _ = v_out_ref.shape
    tokens = length // planes
    for plane in range(planes):
        base = plane * tokens
        first = acc_ref[base : base + kept]
        second = acc_ref[base + kept : base + tokens]
        second = jnp.concatenate([second, first[: 2 * kept - tokens]], axis=0)
        v_out_ref[plane] = jnp.where(low_lanes(first.shape), first, rolled(second)).astype(
            jnp.bfloat16
        )


def unpack_value_kernel(x_ref, out_ref):
    heads, kept, _ = x_ref.shape
    rest = out_ref.shape[0] - kept
    low = low_lanes((kept, LANES))
    for pair in range(heads // 2):
        first = x_ref[2 * pair].astype(jnp.float32)
        second = x_ref[2 * pair + 1].astype(jnp.float32)
        top = jnp.where(low, first, rolled(second))
        bottom = jnp.where(low, rolled(first), second)[:rest]
        out_ref[:, pair * LANES : (pair + 1) * LANES] = jnp.concatenate(
            [top, bottom], axis=0
        ).astype(jnp.bfloat16)


def unpack_pair_kernel(x_ref, q_ref, k_ref):
    heads, tokens, _ = x_ref.shape
    low = low_lanes((tokens, LANES))
    for pair in range(heads // 2):
        first = x_ref[2 * pair].astype(jnp.float32)
        second = x_ref[2 * pair + 1].astype(jnp.float32)
        cols = slice(pair * LANES, (pair + 1) * LANES)
        q_ref[:, cols] = jnp.where(low, first, rolled(second)).astype(jnp.bfloat16)
        k_ref[:, cols] = jnp.where(low, rolled(first), second).astype(jnp.bfloat16)


def exchanged(x, axis):
    return lax.all_to_all(x, axis, split_axis=0, concat_axis=0, tiled=True)


def shaped(*shape, dtype=jnp.bfloat16):
    return jax.ShapeDtypeStruct(shape, dtype)


def shards(inputs, query_vectors, key_vectors, value_vectors, cotangent, gate_prefix, value_weight):
    planes = lax.axis_size("sp")
    tokens, model = inputs.shape[1:]
    width = query_vectors.shape[2]
    heads = width // HEAD_DIM
    length = planes * tokens
    w_cols = value_weight.shape[1]
    packed = pl.pallas_call(
        pack_kernel, out_shape=shaped(heads, tokens + w_cols // 2, 2 * LANES)
    )(query_vectors[0], key_vectors[0], value_vectors[0], cotangent[0], value_weight.T)
    arrived = exchanged(packed, "sp")
    weight_block = pl.pallas_call(unpack_weight_kernel, out_shape=shaped(w_cols, model))(
        arrived[:, tokens:]
    )
    weight_all = lax.all_gather(weight_block, "dp", axis=0, tiled=True)
    kept = (tokens // 2 + 7) // 8 * 8
    pair_grad, value_grad = pl.pallas_call(
        attention_kernel,
        out_shape=(shaped(length, LANES), shaped(planes, kept, LANES)),
        scratch_shapes=[
            pltpu.VMEM((length, LANES), jnp.bfloat16),
            pltpu.VMEM((HEAD_DIM, length), jnp.bfloat16),
            pltpu.VMEM((length, LANES), jnp.float32),
            pltpu.VMEM((length, LANES), jnp.float32),
            pltpu.VMEM((length, LANES), jnp.float32),
            pltpu.VMEM((length, TILE), jnp.float32),
            pltpu.VMEM((length, TILE), jnp.float32),
        ],
    )(arrived[:, :tokens].reshape(length, 2 * LANES), gate_prefix[0])
    value_back = exchanged(value_grad, "sp")
    value_rows = pl.pallas_call(unpack_value_kernel, out_shape=shaped(tokens, width))(value_back)
    partial = lax.dot_general(
        value_rows, inputs[0], (((0,), (0,)), ((), ())), preferred_element_type=jnp.float32
    ).astype(jnp.bfloat16)
    partial = exchanged(partial, "dp").reshape(lax.axis_size("dp"), w_cols, model)
    partial = partial.astype(jnp.float32).sum(axis=0).astype(jnp.bfloat16)
    partial = jnp.moveaxis(partial.reshape(w_cols, planes, model // planes), 1, 0)
    weight_grad = exchanged(partial, "sp").astype(jnp.float32).sum(axis=0).T
    pair_back = exchanged(pair_grad.reshape(planes, tokens, LANES), "sp")
    query_grad, key_grad = pl.pallas_call(
        unpack_pair_kernel, out_shape=(shaped(tokens, width), shaped(tokens, width))
    )(pair_back)
    input_grad = lax.dot_general(
        value_rows, weight_all, (((1,), (0,)), ((), ())), preferred_element_type=jnp.float32
    ).astype(jnp.bfloat16)
    return (query_grad[None], key_grad[None], input_grad[None], weight_grad)


def solution(mesh):
    in_specs = (P("dp", "sp", None),) * 6 + (P("sp", "dp"),)
    out_specs = (P("dp", "sp", None), P("dp", "sp", None), P("dp", "sp", None), P("sp", "dp"))
    return jax.shard_map(shards, mesh=mesh, in_specs=in_specs, out_specs=out_specs, check_vma=False)
```

time: 372 us -> 266 us (0.72)
  the two profiles are of different devices: /device:TPU:32 before, /device:TPU:2 now
where the time goes in v1:
time: 266 us; the launch traced here: 265 us
  blocking collectives  142 us (53%)
  waiting for transfers between devices  56.4 us (21%)
  Pallas kernels  21.3 us (8%)
  starting transfers between devices  18.7 us (7%)
  between operations  14.1 us (5%)
  matrix products  6.03 us (2%)
  other arithmetic  3.59 us (1%)
  local copies, waits for them, and re-layouts  3.16 us (1%)
    all_to_all x2, blocking collectives, exchanged(): return lax.all_to_all(x, axis, split_axis=0, concat_axis=0, tiled=True)  142 us
    all_to_all x3, waiting for transfers between devices, exchanged(): return lax.all_to_all(x, axis, split_axis=0, concat_axis=0, tiled=True)  56.4 us
    all_to_all x3, starting transfers between devices, exchanged(): return lax.all_to_all(x, axis, split_axis=0, concat_axis=0, tiled=True)  18.6 us
    pallas_call x1, Pallas kernels, shards(): pl.pallas_call(attention_kernel, out_shape=(shaped(length, LANES), shaped...  13 us
  transfers between devices with their start and end apart: 4, of which 3 were waited for; matrix products, arithmetic and copies ran while one was open for 3% of the time, Pallas kernels for 2%

profile of v1, /device:TPU:2, one launch (start us, length us, event | category | flops | bytes accessed | tf_op | source)
XLA Modules:
  0.0 265.2 jit_solution(2361466125854040493)
XLA Ops:
  7.2 0.0 copy-start
  7.2 2.8 %shard_map.102 = bf16[16,152,256]{2,1,0:T(8,128)(2,1)} custom-call(bf16[136,1024]{1,0:T(8,128)(2,1)} %bitcast.28, bf16[136,1024]{1,0:T(8,128)(2,1)} %bitcast.29, bf16[136,1024]{1,0:T(8,128)(2,1)} %bitcast.30, bf16[136,1024]{1,0:T(8,128)(2,1)} %bitcast.31, bf16[32,128]{1,0:T(8,128)(2,1)} %bitcast.34), custom_call_target="tpu_custom_call" | custom-call | tf_op jit(solution)/shard_map/pallas_call | solution.py:184
  10.0 76.3 %all_to_all.29 = bf16[16,152,256]{2,1,0:T(8,128)(2,1)S(1)} all-to-all(bf16[16,152,256]{2,1,0:T(8,128)(2,1)} %shard_map.102), channel_id=1, replica_groups=mesh['sp'=16,'dp'=32] {'sp'}, dimensions={0} | all-to-all | bytes 2490368 | tf_op jit(solution)/shard_map/all_to_all | solution.py:170
  86.3 1.1 slice.8
  87.4 13.0 %shard_map.103 = (bf16[2176,128]{1,0:T(8,128)(2,1)}, bf16[16,72,128]{2,1,0:T(8,128)(2,1)}) custom-call(bf16[2176,256]{1,0:T(8,128)(2,1)} %bitcast.25, f32[1,2176]{1,0:T(1,128)} %bitcast.33), custom_call_target="tpu_custom_call" | custom-call | tf_op jit(solution)/shard_map/pallas_call | solution.py:193
  100.4 5.3 %all-to-all-start.2 = ((bf16[16,72,128]{2,1,0:T(8,128)(2,1)}), bf16[16,72,128]{2,1,0:T(8,128)(2,1)S(1)}, u32[]{:S(2)}, u32[]{:S(2)}) async-start(bf16[16,72,128]{2,1,0:T(8,128)(2,1)} %get-tuple-element.11), calls=%async_computation.2 | async-start | bytes 589824 | tf_op jit(solution)/shard_map/all_to_all | solution.py:170
  105.7 0.0 all-gather.2.cloned.1.call-start
  105.8 0.7 slice.9.x_ref
  106.4 1.6 shard_map.106
  108.0 0.0 all-gather.2.cloned.1.call-update
  108.0 17.4 %all-to-all-done.2.x_ref = bf16[16,72,128]{2,1,0:T(8,128)(2,1)S(1)} async-done(((bf16[16,72,128]{2,1,0:T(8,128)(2,1)}), bf16[16,72,128]{2,1,0:T(8,128)(2,1)S(1)}, u32[]{:S(2)}, u32[]{:S(2)}) %all-to-all-start.2) | async-done | bytes 294944 | tf_op jit(solution)/shard_map/all_to_all | solution.py:170
  125.5 0.7 copy-done.3
  126.2 1.9 shard_map.105
  128.0 2.3 convolution_convert_fusion
  130.3 65.7 %all_to_all.30 = bf16[32,32,2048]{2,1,0:T(8,128)(2,1)} all-to-all(bf16[32,32,2048]{2,1,0:T(8,128)(2,1)S(1)} %bitcast.24), channel_id=1, replica_groups=mesh['sp'=16,'dp'=32] {'dp'}, dimensions={0} | all-to-all | bytes 8388608 | tf_op jit(solution)/shard_map/all_to_all | solution.py:170
  196.0 6.1 %all-to-all-start.1 = ((bf16[16,136,128]{2,1,0:T(8,128)(2,1)}), bf16[16,136,128]{2,1,0:T(8,128)(2,1)S(1)}, u32[]{:S(2)}, u32[]{:S(2)}) async-start(bf16[16,136,128]{2,1,0:T(8,128)(2,1)} %bitcast.7), calls=%async_computation.1 | async-start | bytes 1114112 | tf_op jit(solution)/shard_map/all_to_all | solution.py:170
  202.1 3.0 %reduce_sum.21 = bf16[32,2048]{1,0:T(8,128)(2,1)S(1)} reduce(bf16[32,32,2048]{2,1,0:T(8,128)(2,1)} %all_to_all.30, bf16[]{:T(256)} %constant.2.clone.1), dimensions={0}, to_apply=%region_0.0 | reduce | flops 2031616 | bytes 4325378 | tf_op jit(solution)/shard_map/reduce_sum | solution.py:212
  205.1 0.7 copy.11
  205.8 26.4 %all-to-all-done.1.x_ref = bf16[16,136,128]{2,1,0:T(8,128)(2,1)S(1)} async-done(((bf16[16,136,128]{2,1,0:T(8,128)(2,1)}), bf16[16,136,128]{2,1,0:T(8,128)(2,1)S(1)}, u32[]{:S(2)}, u32[]{:S(2)}) %all-to-all-start.1) | async-done | bytes 557088 | tf_op jit(solution)/shard_map/all_to_all | solution.py:170
  232.2 7.2 %all-to-all-start.4 = ((bf16[16,32,128]{2,1,0:T(8,128)(2,1)}), bf16[16,32,128]{2,1,0:T(8,128)(2,1)S(1)}, u32[]{:S(2)}, u32[]{:S(2)}) async-start(bf16[16,32,128]{2,1,0:T(8,128)(2,1)} %copy.11), calls=%async_computation.4 | async-start | bytes 262144 | tf_op jit(solution)/shard_map/all_to_all | solution.py:170
  239.4 2.1 shard_map.104
  241.5 12.5 %all-to-all-done.4 = bf16[16,32,128]{2,1,0:T(8,128)(2,1)S(1)} async-done(((bf16[16,32,128]{2,1,0:T(8,128)(2,1)}), bf16[16,32,128]{2,1,0:T(8,128)(2,1)S(1)}, u32[]{:S(2)}, u32[]{:S(2)}) %all-to-all-start.4) | async-done | bytes 131104 | tf_op jit(solution)/shard_map/all_to_all | solution.py:170
  254.0 0.6 convert_reduce_fusion
  254.6 3.7 %fusion = bf16[1,136,2048]{2,1,0:T(8,128)(2,1)} fusion(bf16[136,1024]{1,0:T(8,128)(2,1)S(1)} %copy-done.1, bf16[1024,2048]{1,0:T(8,128)(2,1)} %all-gather.2.cloned.1.call-done), kind=kOutput, calls=%fused_computation.2 | convolution fusion | flops 570703872 | bytes 5029888 | tf_op jit(solution)/shard_map/dot_general | solution.py:219
  (8 shorter events, 0.0 us)
Async XLA Ops:
  7.2 120.9 %copy-start = (bf16[1,136,2048]{2,1,0:T(8,128)(2,1)S(1)}, bf16[1,136,2048]{2,1,0:T(8,128)(2,1)}, u32[]{:S(2)}) copy-start(bf16[1,136,2048]{2,1,0:T(8,128)(2,1)} %param.7) | copy-start | bytes 1671172
  100.4 25.1 %all-to-all-start.2 = ((bf16[16,72,128]{2,1,0:T(8,128)(2,1)}), bf16[16,72,128]{2,1,0:T(8,128)(2,1)S(1)}, u32[]{:S(2)}, u32[]{:S(2)}) async-start(bf16[16,72,128]{2,1,0:T(8,128)(2,1)} %get-tuple-element.11), calls=%async_computation.2 | async-start | bytes 589824 | tf_op jit(solution)/shard_map/all_to_all | solution.py:170
  105.7 148.9 %all-gather.2.cloned.1.call-start = ((), (), s32[]{:S(2)}) async-start(), calls=%async_computation.5 | async-start | bytes 4325376 | tf_op jit(solution)/shard_map/all_gather | solution.py:191
  125.5 0.7 copy-start.3
  196.0 58.7 %copy-start.1 = (bf16[136,1024]{1,0:T(8,128)(2,1)S(1)}, bf16[136,1024]{1,0:T(8,128)(2,1)}, u32[]{:S(2)}) copy-start(bf16[136,1024]{1,0:T(8,128)(2,1)} %shard_map.105) | copy-start | bytes 835588
  196.0 36.2 %all-to-all-start.1 = ((bf16[16,136,128]{2,1,0:T(8,128)(2,1)}), bf16[16,136,128]{2,1,0:T(8,128)(2,1)S(1)}, u32[]{:S(2)}, u32[]{:S(2)}) async-start(bf16[16,136,128]{2,1,0:T(8,128)(2,1)} %bitcast.7), calls=%async_computation.1 | async-start | bytes 1114112 | tf_op jit(solution)/shard_map/all_to_all | solution.py:170
  232.2 7.2 %copy-start.2 = (bf16[16,136,128]{2,1,0:T(8,128)(2,1)}, bf16[16,136,128]{2,1,0:T(8,128)(2,1)S(1)}, u32[]{:S(2)}) copy-start(bf16[16,136,128]{2,1,0:T(8,128)(2,1)S(1)} %all-to-all-done.1.x_ref) | copy-start | bytes 1671172
  232.2 21.8 %all-to-all-start.4 = ((bf16[16,32,128]{2,1,0:T(8,128)(2,1)}), bf16[16,32,128]{2,1,0:T(8,128)(2,1)S(1)}, u32[]{:S(2)}, u32[]{:S(2)}) async-start(bf16[16,32,128]{2,1,0:T(8,128)(2,1)} %copy.11), calls=%async_computation.4 | async-start | bytes 262144 | tf_op jit(solution)/shard_map/all_to_all | solution.py:170
Sparse Core Ops, SparseCore 0:
  109.7 86.0 all-gather.1
